TPU v7x, 128 devices: a 2x2x16 block of a 8x8x16 slice. The times are simulated.
128 devices in a mesh: grp: 4 (over y, x), ep: 32 (over z, core).
Axes of the slice: x: 2, y: 2, z: 16, core: 2. Of those that a mesh axis runs over, the one named last changes fastest.
The devices are a block of a 8x8x16 slice.
Arguments:
- tokens: bfloat16 [2048, 2048], P(('grp', 'ep')), parts along dimension 0, may hold values from -6 to 6
- norm_gain: bfloat16 [2048], replicated, may hold values from 0.099609375 to 1.8984375
- query_weight: bfloat16 [2048, 1024], P(None, 'ep'), may hold values from -0.125 to 0.125
- key_weight: bfloat16 [2048, 256], replicated, may hold values from -0.25 to 0.25
- value_weight: bfloat16 [2048, 256], replicated, may hold values from -0.125 to 0.125
- out_weight: bfloat16 [1024, 2048], P(None, 'ep'), may hold values from -0.1875 to 0.1875
- head_gain: bfloat16 [128], replicated, may hold values from 0.099609375 to 1.8984375
- lambdas: float32 [8], replicated, may hold values from 0.3 to 0.8
- cache_keys: bfloat16 [2048, 1024, 2, 128], P(('grp', 'ep')), parts along dimension 0, may hold values from -1000 to 1000
- cache_values: bfloat16 [2048, 1024, 2, 128], P(('grp', 'ep')), parts along dimension 0, may hold values from -6 to 6
- lengths: int32 [2048], P(('grp', 'ep')), parts along dimension 0, may hold values from 64 to 1024
- moe_gain: bfloat16 [2048], replicated, may hold values from 0.099609375 to 1.8984375
- gate_weight: bfloat16 [32, 2048, 1024], P('ep'), may hold values from -0.375 to 0.375
- up_weight: bfloat16 [32, 2048, 1024], P('ep'), may hold values from -0.375 to 0.375
- down_weight: bfloat16 [32, 1024, 2048], P('ep'), may hold values from -0.02734375 to 0.02734375
- routes: int32 [2048, 4], P(('grp', 'ep')), parts along dimension 0, may hold values from 0 to 31, all different within a row; in each aligned block of 16 rows (0 to 15, 16 to 31, ...) at most 4 rows name the same one
- route_weights: float32 [2048, 4], P(('grp', 'ep')), parts along dimension 0, may hold values from 0.2 to 1
Outputs:
- mixed: bfloat16 [2048, 2048], P(('grp', 'ep')), parts along dimension 0
There are 4 independent parts, one for each index of `grp`. A program takes and returns all parts, laid end to end along the dimension named above; an argument that names none is the same for every part. Nothing has to cross between parts.
Inputs may be any that keep to these rules, and one draw needn't show every extreme that they name: `routes`: a token's 4 experts differ; the tokens of one device name each expert at most 4 times, and in every draw some expert is named exactly 4 times by one device's tokens.
All inputs are finite; a program needn't handle non-finite values.
Results may differ from a plain program's by a relative error of at most 0.034.
Values may be sent and summed in bfloat16 or wider, within the bound.
A program may use at most 128 MiB of HBM per device.

v0:
```python
import jax
import jax.numpy as jnp
from jax import lax
from jax.sharding import Mesh
from jax.sharding import PartitionSpec as P

EP = ("ep_0", "ep_1")
GRP_EP = ("grp", "ep_0", "ep_1")
epsilon = 1e-06
masked_score = -1e30
clamp_limit = 7.0
swish_alpha = 1.702


def in_blocks(value, dim, length):
    before, after = (value.shape[:dim], value.shape[dim + 1 :])
    return jnp.moveaxis(value.reshape(*before, length, -1, *after), dim, 0)


def joined_along(blocks, dim):
    blocks = jnp.moveaxis(blocks, 0, dim)
    lengths = blocks.shape
    return blocks.reshape(*lengths[:dim], lengths[dim] * lengths[dim + 1], *lengths[dim + 2 :])


def moved_by_axis(blocks, axes, sequence):
    inside = blocks.shape[1:]
    filled = blocks.reshape(*(lax.axis_size(a) for a in axes), *inside)
    for k in sequence:
        filled = lax.all_to_all(filled, axes[k], k, k, tiled=True)
    return filled.reshape(-1, *inside)


def two_step_exchange(value, groups, sequence, split_dim, concat_dim):
    length = lax.axis_size(groups[0]) * lax.axis_size(groups[1])
    blocks = in_blocks(value, split_dim, length)
    return joined_along(moved_by_axis(blocks, groups, sequence), concat_dim)


def rms_scaled(values, gain):
    floats = values.astype(jnp.float32)
    return (
        floats
        * lax.rsqrt(jnp.mean(floats * floats, axis=-1, keepdims=True) + epsilon)
        * gain.astype(jnp.float32)
    )


def attention(queries, new_keys, new_values, cache_keys, cache_values, lengths, lambdas, head_gain):
    count = queries.shape[0]
    ctx_len = cache_keys.shape[1]
    kv_count = cache_keys.shape[2]
    head_dim = cache_keys.shape[3] // 2
    heads = lambdas.shape[0]
    group = heads // kv_count
    val_dim = cache_values.shape[3]
    query_grid = queries.reshape(count, kv_count, group, 2, head_dim)
    key_grid = cache_keys.reshape(count, ctx_len, kv_count, 2, head_dim)
    own_keys = new_keys.reshape(count, kv_count, 2, head_dim)
    inv_scale = head_dim ** (-0.5)
    scores = (
        jnp.einsum("bkgcd,bjkcd->bkgcj", query_grid, key_grid, preferred_element_type=jnp.float32)
        * inv_scale
    )
    own_score = (
        jnp.einsum("bkgcd,bkcd->bkgc", query_grid, own_keys, preferred_element_type=jnp.float32)
        * inv_scale
    )
    visible = jnp.arange(ctx_len, dtype=jnp.int32)[None, :] < lengths[:, None]
    scores = jnp.where(visible[:, None, None, None, :], scores, masked_score)
    highest = jnp.maximum(jnp.max(scores, axis=-1), own_score)
    expd = jnp.exp(scores - highest[..., None])
    own_exp = jnp.exp(own_score - highest)
    denominator = jnp.sum(expd, axis=-1) + own_exp
    probs = expd / denominator[..., None]
    own_prob = own_exp / denominator
    lambda_grid = lambdas.reshape(kv_count, group)[None, :, :]
    weights = (probs[:, :, :, 0] - lambda_grid[..., None] * probs[:, :, :, 1]).astype(jnp.bfloat16)
    own_weight = (own_prob[..., 0] - lambda_grid * own_prob[..., 1]).astype(jnp.bfloat16)
    attended = jnp.einsum(
        "bkgj,bjkv->bkgv", weights, cache_values, preferred_element_type=jnp.float32
    )
    own_vals = new_values.reshape(count, kv_count, val_dim).astype(jnp.float32)
    attended = attended + own_weight.astype(jnp.float32)[..., None] * own_vals[:, :, None, :]
    return rms_scaled(attended, head_gain).reshape(count, heads * val_dim).astype(jnp.bfloat16)


def expert_mlp(inputs, gate_w, up_w, down_w):
    gate = jnp.dot(inputs, gate_w, preferred_element_type=jnp.float32)
    upper = jnp.dot(inputs, up_w, preferred_element_type=jnp.float32)
    gate = jnp.minimum(gate, clamp_limit)
    upper = jnp.clip(upper, -clamp_limit, clamp_limit)
    act = ((upper + 1.0) * gate * jax.nn.sigmoid(swish_alpha * gate)).astype(jnp.bfloat16)
    return jnp.dot(act, down_w, preferred_element_type=jnp.float32).astype(jnp.bfloat16)


def local(
    tokens,
    norm_gain,
    query_weight,
    key_weight,
    value_weight,
    out_weight,
    head_gain,
    lambdas,
    cache_keys,
    cache_values,
    lengths,
    moe_gain,
    gate_weight,
    up_weight,
    down_weight,
    routes,
    route_weights,
):
    count = tokens.shape[0]
    width = tokens.shape[1]
    topk = routes.shape[1]
    normed = rms_scaled(tokens, norm_gain).astype(jnp.bfloat16)
    new_keys = jnp.dot(normed, key_weight, preferred_element_type=jnp.float32).astype(jnp.bfloat16)
    new_values = jnp.dot(normed, value_weight, preferred_element_type=jnp.float32).astype(
        jnp.bfloat16
    )
    queries = jnp.dot(
        normed,
        lax.all_gather(query_weight, EP, axis=1, tiled=True),
        preferred_element_type=jnp.float32,
    ).astype(jnp.bfloat16)
    head_out = attention(
        queries, new_keys, new_values, cache_keys, cache_values, lengths, lambdas, head_gain
    )
    attn_out = jnp.dot(
        head_out,
        lax.all_gather(out_weight, EP, axis=1, tiled=True),
        preferred_element_type=jnp.float32,
    ).astype(jnp.bfloat16)
    residual = (tokens.astype(jnp.float32) + attn_out.astype(jnp.float32)).astype(jnp.bfloat16)
    moe_in = rms_scaled(residual, moe_gain).astype(jnp.bfloat16)
    experts = lax.axis_size(EP)
    capacity = min(count, max(2, 2 * count * topk // experts))
    onehot = (routes.reshape(-1)[:, None] == jnp.arange(experts, dtype=jnp.int32)[None, :]).astype(
        jnp.int32
    )
    earlier_all = jnp.cumsum(onehot, axis=0) - onehot
    ranks = jnp.sum(earlier_all * onehot, axis=1).reshape(count, topk)
    slot_id = routes * capacity + ranks
    slot_range = jnp.arange(experts * capacity, dtype=jnp.int32)
    dispatch = jnp.any(slot_id[None, :, :] == slot_range[:, None, None], axis=2).astype(
        jnp.bfloat16
    )
    outgoing = jnp.dot(dispatch, moe_in, preferred_element_type=jnp.float32).astype(jnp.bfloat16)
    outgoing = outgoing.reshape(experts, capacity, width)
    received = lax.all_to_all(outgoing, EP, split_axis=0, concat_axis=0, tiled=True)
    flat_rows = received.reshape(-1, width)
    results = expert_mlp(flat_rows, gate_weight[0], up_weight[0], down_weight[0]).reshape(
        received.shape
    )
    returned = two_step_exchange(results, ("ep_0", "ep_1"), (1, 0), 0, 0)
    picked = returned.reshape(-1, width)[slot_id].astype(jnp.float32)
    moe_sum = jnp.sum(route_weights[:, :, None] * picked, axis=1)
    return (residual.astype(jnp.float32) + moe_sum).astype(jnp.bfloat16)


def solution(mesh):
    torus = Mesh(mesh.devices.reshape(mesh.shape["grp"], 16, 2), ("grp", "ep_0", "ep_1"))
    return jax.shard_map(
        local,
        mesh=torus,
        in_specs=(
            P(GRP_EP, None),
            P(),
            P(None, EP),
            P(),
            P(),
            P(None, EP),
            P(),
            P(),
            P(GRP_EP, None, None, None),
            P(GRP_EP, None, None, None),
            P(GRP_EP),
            P(),
            P(EP, None, None),
            P(EP, None, None),
            P(EP, None, None),
            P(GRP_EP, None),
            P(GRP_EP, None),
        ),
        out_specs=P(GRP_EP, None),
        check_vma=False,
    )
```

profile of v0, /device:TPU:196, one launch (start us, length us, event | category | flops | bytes accessed | tf_op | source)
XLA Modules:
  0.0 256.7 jit_solution(1029286353424995351)
XLA Ops:
  6.6 0.7 all-gather.3.cloned.1.call-update
  7.4 0.7 all-gather.5.cloned.1.call-update
  8.1 0.7 convert_element_type.86
  8.8 1.0 fusion.57
  9.8 1.1 convolution_convert_fusion.4
  11.1 21.2 %copy.77 = bf16[16,1024,2,128]{1,3,2,0:T(8,128)(2,1)} copy(bf16[16,1024,2,128]{3,2,1,0:T(2,128)(2,1)} %param.25) | data formatting | bytes 16777216 | tf_op args[8]
  33.7 51.4 %all-gather.3.cloned.1.call-done = bf16[2048,1024]{0,1:T(8,128)(2,1)} async-done(((bf16[2048,32]{0,1:T(8,128)(2,1)}), bf16[2048,1024]{0,1:T(8,128)(2,1)}) %all-gather.3.cloned.1.call-update) | async-done | bytes 4194320 | tf_op jit(solution)/shard_map/all_gather | solution.py:126
  85.0 3.4 %convolution_convert_fusion.2 = bf16[16,1024]{1,0:T(8,128)(2,1)S(1)} fusion(bf16[2048,1024]{0,1:T(8,128)(2,1)} %all-gather.3.cloned.1.call-done, bf16[16,2048]{1,0:T(8,128)(2,1)S(1)} %copy-done.1, f32[2048]{0:T(1024)S(1)} %convert_element_type.86, f32[16]{0:T(128)S(1)} %add_rsqrt_fusion.2), kind=kOutput, calls=%fused_computation.26 | convolution fusion | flops 67256320 | bytes 4300864 | tf_op jit(solution)/shard_map/dot_general | solution.py:124
  88.9 4.7 %fusion.81 = (f32[16,2,4,2]{2,3,1,0:T(2,128)S(1)}, f32[16,2,4,2,1024]{4,2,3,1,0:T(4,128)S(1)}) fusion(bf16[16,1024,2,2,64]{1,4,3,2,0:T(8,128)(2,1)} %bitcast.96, bf16[16,2,4,2,64]{4,3,2,1,0:T(2,128)(2,1)S(1)} %reshape.79, pred[16,1024]{1,0:T(8,128)(4,1)S(1)} %iota_compare_fusion), kind=kOutput, calls=%fused_computation.91 | convolution fusion | flops 34340608 | bytes 9487360 | tf_op jit(solution)/shard_map/bkgcd,bjkcd->bkgcj/dot_general | solution.py:62
  93.8 0.5 fusion.40
  94.8 0.5 fusion.39
  95.3 5.0 %multiply_reduce_fusion.2 = (f32[16,2,4]{2,1,0:T(2,128)S(1)}, f32[16,2,4,128]{3,2,1,0:T(4,128)S(1)}) fusion(f32[16,2,128]{2,1,0:T(2,128)S(1)} %reshape.86, f32[16,2,4]{2,1,0:T(2,128)S(1)} %copy.85, bf16[16,1024,2,128]{3,2,1,0:T(2,128)(2,1)} %param.26, f32[16,2,4,2,1024]{4,2,3,1,0:T(4,128)S(1)} %fusion.39, f32[2,4]{1,0:T(2,128)S(1)} %mul.149), kind=kOutput, calls=%fused_computation.60 | convolution fusion | flops 34013056 | bytes 9520160 | tf_op jit(solution)/shard_map/bkgj,bjkv->bkgv/dot_general | solution.py:80
  100.6 53.6 %all-gather.5.cloned.1.call-done = bf16[1024,2048]{0,1:T(8,128)(2,1)} async-done(((bf16[1024,64]{0,1:T(8,128)(2,1)}), bf16[1024,2048]{0,1:T(8,128)(2,1)}) %all-gather.5.cloned.1.call-update) | async-done | bytes 4194320 | tf_op jit(solution)/shard_map/all_gather | solution.py:134
  154.3 3.5 %multiply_reduce_fusion.1 = (f32[16]{0:T(128)S(1)}, f32[16,2048]{1,0:T(8,128)S(1)}) fusion(bf16[16,1024]{1,0:T(8,128)(2,1)S(1)} %convert_element_type.97, bf16[1024,2048]{0,1:T(8,128)(2,1)} %all-gather.5.cloned.1.call-done, bf16[16,2048]{1,0:T(8,128)(2,1)S(1)} %copy-done.1), kind=kOutput, calls=%fused_computation.56 | convolution fusion | flops 67370992 | bytes 4423744 | tf_op jit(solution)/shard_map/dot_general | solution.py:132
  158.3 40.2 %all_to_all.15 = bf16[32,4,2048]{2,1,0:T(4,128)(2,1)S(1)} all-to-all(bf16[32,4,2048]{2,1,0:T(4,128)(2,1)S(1)} %reshape.83), channel_id=1, replica_groups=mesh['grp'=4,'ep_0'=16,'ep_1'=2] {'ep_0','ep_1'}, dimensions={0} | all-to-all | bytes 1048576 | tf_op jit(solution)/shard_map/all_to_all | solution.py:153
  198.7 2.9 %fusion.20 = f32[128,1024]{1,0:T(8,128)S(1)} fusion(bf16[128,2048]{1,0:T(8,128)(2,1)S(1)} %reshape.84, bf16[1,2048,1024]{2,1,0:T(8,128)(2,1)} %param.29), kind=kOutput, calls=%fused_computation.20 | convolution fusion | flops 537001984 | bytes 5242880 | tf_op jit(solution)/shard_map/dot_general | solution.py:89
  201.6 4.9 %fusion.8 = bf16[128,2048]{1,0:T(8,128)(2,1)S(1)} fusion(bf16[1,1024,2048]{2,1,0:T(8,128)(2,1)} %param.31, f32[128,1024]{1,0:T(8,128)S(1)} %fusion.20, bf16[128,2048]{1,0:T(8,128)(2,1)S(1)} %reshape.84, bf16[1,2048,1024]{2,1,0:T(8,128)(2,1)} %param.30), kind=kOutput, calls=%fused_computation.9 | convolution fusion | flops 1075183616 | bytes 9961472 | tf_op jit(solution)/shard_map/dot_general | solution.py:94
  206.9 4.2 %all_to_all.16 = bf16[16,2,1,4,2048]{4,3,0,2,1:T(4,128)(2,1)S(1)} all-to-all(bf16[16,2,1,4,2048]{4,3,0,2,1:T(4,128)(2,1)S(1)} %copy.92), channel_id=1, replica_groups=mesh['grp'=4,'ep_0'=16,'ep_1'=2] {'ep_1'}, dimensions={1} | all-to-all | bytes 1048576 | tf_op jit(solution)/shard_map/all_to_all | solution.py:30
  211.1 1.0 copy.93
  212.1 5.5 %all-to-all-start.2 = ((bf16[16,2,1,4,2048]{4,3,1,2,0:T(4,128)(2,1)}), bf16[16,2,1,4,2048]{4,3,1,2,0:T(4,128)(2,1)S(1)}, u32[]{:S(2)}, u32[]{:S(2)}) async-start(bf16[16,2,1,4,2048]{4,3,1,2,0:T(4,128)(2,1)} %copy.93), calls=%async_computation.2 | async-start | bytes 1048576 | tf_op jit(solution)/shard_map/all_to_all | solution.py:30
  217.9 29.9 %all-to-all-done.2 = bf16[16,2,1,4,2048]{4,3,1,2,0:T(4,128)(2,1)S(1)} async-done(((bf16[16,2,1,4,2048]{4,3,1,2,0:T(4,128)(2,1)}), bf16[16,2,1,4,2048]{4,3,1,2,0:T(4,128)(2,1)S(1)}, u32[]{:S(2)}, u32[]{:S(2)}) %all-to-all-start.2) | async-done | bytes 524320 | tf_op jit(solution)/shard_map/all_to_all | solution.py:30
  247.9 0.7 gather_fusion
  248.8 0.4 multiply_reduce_fusion
  249.2 0.6 add_convert_fusion
  (64 shorter events, 4.4 us)
Async XLA Ops:
  6.5 3.2 %copy-start = (bf16[2048,256]{1,0:T(8,128)(2,1)S(1)}, bf16[2048,256]{1,0:T(8,128)(2,1)}, u32[]{:S(2)}) copy-start(bf16[2048,256]{1,0:T(8,128)(2,1)} %param.20) | copy-start | bytes 3145732
  6.6 78.5 %all-gather.3.cloned.1.call-start = ((), (), s32[]{:S(2)}) async-start(), calls=%async_computation.3 | async-start | bytes 4325376 | tf_op jit(solution)/shard_map/all_gather | solution.py:126
  7.3 147.0 %all-gather.5.cloned.1.call-start = ((), (), s32[]{:S(2)}) async-start(), calls=%async_computation.4 | async-start | bytes 4325376 | tf_op jit(solution)/shard_map/all_gather | solution.py:134
  11.0 21.3 %copy-start.7 = (f32[8]{0:T(128)S(1)}, f32[8]{0:T(128)}, u32[]{:S(2)}) copy-start(f32[8]{0:T(128)} %param.24) | copy-start | bytes 100
  11.0 21.4 %copy-start.1 = (bf16[16,2048]{1,0:T(8,128)(2,1)S(1)}, bf16[16,2048]{1,0:T(8,128)(2,1)}, u32[]{:S(2)}) copy-start(bf16[16,2048]{1,0:T(8,128)(2,1)} %param.17) | copy-start | bytes 196612
  11.0 21.4 %copy-start.2 = (bf16[2048,256]{1,0:T(8,128)(2,1)S(1)}, bf16[2048,256]{1,0:T(8,128)(2,1)}, u32[]{:S(2)}) copy-start(bf16[2048,256]{1,0:T(8,128)(2,1)} %param.21) | copy-start | bytes 3145732
  11.0 21.7 %copy-start.8 = (bf16[128]{0:T(256)(128)(2,1)S(1)}, bf16[128]{0:T(256)(128)(2,1)}, u32[]{:S(2)}) copy-start(bf16[128]{0:T(256)(128)(2,1)} %param.23) | copy-start | bytes 772
  11.1 21.7 %copy-start.4 = (s32[16,4]{0,1:T(4,128)S(1)}, s32[16,4]{0,1:T(4,128)}, u32[]{:S(2)}) copy-start(s32[16,4]{0,1:T(4,128)} %param.32) | copy-start | bytes 772
  11.1 22.4 %copy-start.3 = (bf16[2048]{0:T(1024)(128)(2,1)S(1)}, bf16[2048]{0:T(1024)(128)(2,1)}, u32[]{:S(2)}) copy-start(bf16[2048]{0:T(1024)(128)(2,1)} %param.28) | copy-start | bytes 12292
  11.1 22.5 %copy-start.6 = (s32[16]{0:T(128)S(1)}, s32[16]{0:T(128)}, u32[]{:S(2)}) copy-start(s32[16]{0:T(128)} %param.27) | copy-start | bytes 196
  206.5 11.3 %copy-start.5 = (f32[16,4]{0,1:T(4,128)S(1)}, f32[16,4]{0,1:T(4,128)}, u32[]{:S(2)}) copy-start(f32[16,4]{0,1:T(4,128)} %param.33) | copy-start | bytes 772
  212.1 35.6 %all-to-all-start.2 = ((bf16[16,2,1,4,2048]{4,3,1,2,0:T(4,128)(2,1)}), bf16[16,2,1,4,2048]{4,3,1,2,0:T(4,128)(2,1)S(1)}, u32[]{:S(2)}, u32[]{:S(2)}) async-start(bf16[16,2,1,4,2048]{4,3,1,2,0:T(4,128)(2,1)} %copy.93), calls=%async_computation.2 | async-start | bytes 1048576 | tf_op jit(solution)/shard_map/all_to_all | solution.py:30
Sparse Core Ops, SparseCore 0:
  9.1 75.9 all-gather.2
  86.7 67.4 all-gather.4
where the time goes:
time: 258 us; the launch traced here: 257 us
  waiting for transfers between devices  136 us (53%)
  blocking collectives  44.4 us (17%)
  matrix products  26.3 us (10%)
  local copies, waits for them, and re-layouts  25.8 us (10%)
  between operations  13.7 us (5%)
  starting transfers between devices  5.6 us (2%)
  other arithmetic  4.51 us (2%)
    all_gather x1, waiting for transfers between devices, local(): lax.all_gather(out_weight, EP, axis=1, tiled=True)  53.6 us
    all_gather x1, waiting for transfers between devices, local(): lax.all_gather(query_weight, EP, axis=1, tiled=True)  51.4 us
    all_to_all x1, blocking collectives, local(): lax.all_to_all(outgoing, EP, split_axis=0, concat_axis=0, tiled=True)  40.2 us
    all_to_all x1, waiting for transfers between devices, moved_by_axis(): filled = lax.all_to_all(filled, axes[k], k, k, tiled=True)  29.9 us
    unnamed x21, local copies, waits for them, and re-layouts  21.5 us
    all_to_all x1, starting transfers between devices, moved_by_axis(): filled = lax.all_to_all(filled, axes[k], k, k, tiled=True)  5.54 us
  transfers between devices with their start and end apart: 3, of which 3 were waited for; matrix products, arithmetic and copies ran while one was open for 16% of the time, Pallas kernels for 0%

commit v1 on v0

--- a/solution.py
+++ b/solution.py
@@ -10,6 +10,11 @@
 masked_score = -1e30
 clamp_limit = 7.0
 swish_alpha = 1.702
+
+
+def exchange_gather(array, mesh_axis, dim):
+    sent = jnp.stack([array] * lax.axis_size(mesh_axis))
+    return jnp.concatenate(lax.all_to_all(sent, mesh_axis, 0, 0), axis=dim)
 
 
 def in_blocks(value, dim, length):
@@ -122,9 +127,7 @@
         jnp.bfloat16
     )
     queries = jnp.dot(
-        normed,
-        lax.all_gather(query_weight, EP, axis=1, tiled=True),
-        preferred_element_type=jnp.float32,
+        normed, exchange_gather(query_weight, EP, 1), preferred_element_type=jnp.float32
     ).astype(jnp.bfloat16)
     head_out = attention(
         queries, new_keys, new_values, cache_keys, cache_values, lengths, lambdas, head_gain

time: 258 us -> 352 us (1.36)
  waiting for transfers between devices: 136 us -> 217 us
  starting transfers between devices: 5.6 us -> 22.7 us
  blocking collectives: 44.4 us -> 40.5 us
    all_to_all x0 -> x1, waiting for transfers between devices: none -> 186 us  [exchange_gather(): return jnp.concatenate(lax.all_to_all(sent, mesh_axis, 0, 0), axis=dim)]
    all_gather x1, waiting for transfers between devices: 53.6 us -> 0.02 us  [local(): lax.all_gather(out_weight, EP, axis=1, tiled=True)]
    all_gather x1 -> x0, waiting for transfers between devices: 51.4 us -> none  [local(): lax.all_gather(query_weight, EP, axis=1, tiled=True)]
    all_to_all x0 -> x1, starting transfers between devices: none -> 17.1 us  [exchange_gather(): return jnp.concatenate(lax.all_to_all(sent, mesh_axis, 0, 0), axis=dim)]
    all_to_all x1, blocking collectives: 40.2 us -> 36.4 us  [local(): lax.all_to_all(outgoing, EP, split_axis=0, concat_axis=0, tiled=True)]
    unnamed x21 -> x23, local copies, waits for them, and re-layouts: 21.5 us -> 21.5 us
  transfers between devices with their start and end apart: 3 -> 3, of which waited for: 3 -> 2; matrix products, arithmetic and copies ran while one was open for 16% -> 11% of each run, Pallas kernels for 0% -> 0%
where the time goes in v1:
time: 352 us; the launch traced here: 351 us
  waiting for transfers between devices  217 us (62%)
  blocking collectives  40.5 us (12%)
  local copies, waits for them, and re-layouts  29.2 us (8%)
  matrix products  25.4 us (7%)
  starting transfers between devices  22.7 us (6%)
  between operations  13.7 us (4%)
    all_to_all x1, waiting for transfers between devices, exchange_gather(): return jnp.concatenate(lax.all_to_all(sent, mesh_axis, 0, 0), axis=dim)  186 us
    all_to_all x1, blocking collectives, local(): lax.all_to_all(outgoing, EP, split_axis=0, concat_axis=0, tiled=True)  36.4 us
    all_to_all x1, waiting for transfers between devices, moved_by_axis(): filled = lax.all_to_all(filled, axes[k], k, k, tiled=True)  29.9 us
    unnamed x23, local copies, waits for them, and re-layouts  21.5 us
    all_to_all x1, starting transfers between devices, exchange_gather(): return jnp.concatenate(lax.all_to_all(sent, mesh_axis, 0, 0), axis=dim)  17.1 us
  transfers between devices with their start and end apart: 3, of which 2 were waited for; matrix products, arithmetic and copies ran while one was open for 11% of the time, Pallas kernels for 0%

profile of v1, /device:TPU:196, one launch (start us, length us, event | category | flops | bytes accessed | tf_op | source)
XLA Modules:
  0.0 351.2 jit_solution(16886126520471001034)
XLA Ops:
  6.6 3.4 stack.2
  10.0 17.1 %all-to-all-start = ((bf16[32,2048,32]{1,2,0:T(8,128)(2,1)}), bf16[32,2048,32]{1,2,0:T(8,128)(2,1)}, u32[]{:S(2)}, u32[]{:S(2)}) async-start(bf16[32,2048,32]{1,2,0:T(8,128)(2,1)} %stack.2), calls=%async_computation | async-start | bytes 8388608 | tf_op jit(solution)/shard_map/all_to_all | solution.py:17
  27.2 0.7 all-gather.2.cloned.1.call-update
  28.1 0.3 convolution_convert_fusion.4
  28.6 21.3 %copy.78 = bf16[16,1024,2,128]{1,3,2,0:T(8,128)(2,1)} copy(bf16[16,1024,2,128]{3,2,1,0:T(2,128)(2,1)} %param.25) | data formatting | bytes 16777216 | tf_op args[8]
  49.9 0.3 fusion.38
  51.2 186.0 %all-to-all-done = bf16[32,2048,32]{1,2,0:T(8,128)(2,1)} async-done(((bf16[32,2048,32]{1,2,0:T(8,128)(2,1)}), bf16[32,2048,32]{1,2,0:T(8,128)(2,1)}, u32[]{:S(2)}, u32[]{:S(2)}) %all-to-all-start) | async-done | bytes 4194336 | tf_op jit(solution)/shard_map/all_to_all | solution.py:17
  237.2 3.4 convolution_convert_fusion.2
  241.0 4.7 %fusion.81 = (f32[16,2,4,2]{2,3,1,0:T(2,128)S(1)}, f32[16,2,4,2,1024]{4,2,3,1,0:T(4,128)S(1)}) fusion(bf16[16,1024,2,2,64]{1,4,3,2,0:T(8,128)(2,1)} %bitcast.99, bf16[16,2,4,2,64]{4,3,2,1,0:T(2,128)(2,1)S(1)} %reshape.89, pred[16,1024]{1,0:T(8,128)(4,1)S(1)} %iota_compare_fusion), kind=kOutput, calls=%fused_computation.91 | convolution fusion | flops 34340608 | bytes 9487360 | tf_op jit(solution)/shard_map/bkgcd,bjkcd->bkgcj/dot_general | solution.py:67
  245.9 0.5 fusion.40
  246.9 0.5 fusion.39
  247.4 4.9 %multiply_reduce_fusion.2 = (f32[16,2,4]{2,1,0:T(2,128)S(1)}, f32[16,2,4,128]{3,2,1,0:T(4,128)S(1)}) fusion(f32[16,2,128]{2,1,0:T(2,128)S(1)} %reshape.96, f32[16,2,4]{2,1,0:T(2,128)S(1)} %copy.86, bf16[16,1024,2,128]{3,2,1,0:T(2,128)(2,1)} %param.26, f32[16,2,4,2,1024]{4,2,3,1,0:T(4,128)S(1)} %fusion.39, f32[2,4]{1,0:T(2,128)S(1)} %mul.149), kind=kOutput, calls=%fused_computation.60 | convolution fusion | flops 34013056 | bytes 9520160 | tf_op jit(solution)/shard_map/bkgj,bjkv->bkgv/dot_general | solution.py:85
  252.7 3.5 multiply_reduce_fusion.1
  256.2 0.4 convolution_convert_fusion
  256.7 36.4 %all_to_all.20 = bf16[32,4,2048]{2,1,0:T(4,128)(2,1)S(1)} all-to-all(bf16[32,4,2048]{2,1,0:T(4,128)(2,1)S(1)} %reshape.93), channel_id=1, replica_groups=mesh['grp'=4,'ep_0'=16,'ep_1'=2] {'ep_0','ep_1'}, dimensions={0} | all-to-all | bytes 1048576 | tf_op jit(solution)/shard_map/all_to_all | solution.py:156
  293.2 2.9 fusion.20
  296.2 4.9 %fusion.8 = bf16[128,2048]{1,0:T(8,128)(2,1)S(1)} fusion(bf16[1,1024,2048]{2,1,0:T(8,128)(2,1)} %param.31, f32[128,1024]{1,0:T(8,128)S(1)} %fusion.20, bf16[128,2048]{1,0:T(8,128)(2,1)S(1)} %reshape.94, bf16[1,2048,1024]{2,1,0:T(8,128)(2,1)} %param.30), kind=kOutput, calls=%fused_computation.9 | convolution fusion | flops 1075183616 | bytes 9961472 | tf_op jit(solution)/shard_map/dot_general | solution.py:99
  301.5 4.2 %all_to_all.21 = bf16[16,2,1,4,2048]{4,3,0,2,1:T(4,128)(2,1)S(1)} all-to-all(bf16[16,2,1,4,2048]{4,3,0,2,1:T(4,128)(2,1)S(1)} %copy.93), channel_id=1, replica_groups=mesh['grp'=4,'ep_0'=16,'ep_1'=2] {'ep_1'}, dimensions={1} | all-to-all | bytes 1048576 | tf_op jit(solution)/shard_map/all_to_all | solution.py:35
  305.7 1.0 copy.94
  306.7 5.5 %all-to-all-start.3 = ((bf16[16,2,1,4,2048]{4,3,1,2,0:T(4,128)(2,1)}), bf16[16,2,1,4,2048]{4,3,1,2,0:T(4,128)(2,1)S(1)}, u32[]{:S(2)}, u32[]{:S(2)}) async-start(bf16[16,2,1,4,2048]{4,3,1,2,0:T(4,128)(2,1)} %copy.94), calls=%async_computation.3 | async-start | bytes 1048576 | tf_op jit(solution)/shard_map/all_to_all | solution.py:35
  312.4 29.9 %all-to-all-done.3 = bf16[16,2,1,4,2048]{4,3,1,2,0:T(4,128)(2,1)S(1)} async-done(((bf16[16,2,1,4,2048]{4,3,1,2,0:T(4,128)(2,1)}), bf16[16,2,1,4,2048]{4,3,1,2,0:T(4,128)(2,1)S(1)}, u32[]{:S(2)}, u32[]{:S(2)}) %all-to-all-start.3) | async-done | bytes 524320 | tf_op jit(solution)/shard_map/all_to_all | solution.py:35
  342.4 0.7 gather_fusion
  343.3 0.4 multiply_reduce_fusion
  343.7 0.6 add_convert_fusion
  (66 shorter events, 3.9 us)
Async XLA Ops:
  6.5 21.6 %copy-start = (bf16[2048,256]{1,0:T(8,128)(2,1)S(1)}, bf16[2048,256]{1,0:T(8,128)(2,1)}, u32[]{:S(2)}) copy-start(bf16[2048,256]{1,0:T(8,128)(2,1)} %param.20) | copy-start | bytes 3145732
  10.0 18.0 %copy-start.3 = (bf16[2048]{0:T(1024)(128)(2,1)S(1)}, bf16[2048]{0:T(1024)(128)(2,1)}, u32[]{:S(2)}) copy-start(bf16[2048]{0:T(1024)(128)(2,1)} %param.18) | copy-start | bytes 12292
  10.0 18.0 %copy-start.1 = (bf16[16,2048]{1,0:T(8,128)(2,1)S(1)}, bf16[16,2048]{1,0:T(8,128)(2,1)}, u32[]{:S(2)}) copy-start(bf16[16,2048]{1,0:T(8,128)(2,1)} %param.17) | copy-start | bytes 196612
  10.0 227.2 %all-to-all-start = ((bf16[32,2048,32]{1,2,0:T(8,128)(2,1)}), bf16[32,2048,32]{1,2,0:T(8,128)(2,1)}, u32[]{:S(2)}, u32[]{:S(2)}) async-start(bf16[32,2048,32]{1,2,0:T(8,128)(2,1)} %stack.2), calls=%async_computation | async-start | bytes 8388608 | tf_op jit(solution)/shard_map/all_to_all | solution.py:17
  27.1 225.5 %all-gather.2.cloned.1.call-start = ((), (), s32[]{:S(2)}) async-start(), calls=%async_computation.4 | async-start | bytes 4325376 | tf_op jit(solution)/shard_map/all_gather | solution.py:137
  28.5 21.3 %copy-start.8 = (f32[8]{0:T(128)S(1)}, f32[8]{0:T(128)}, u32[]{:S(2)}) copy-start(f32[8]{0:T(128)} %param.24) | copy-start | bytes 100
  28.5 21.4 %copy-start.2 = (bf16[2048,256]{1,0:T(8,128)(2,1)S(1)}, bf16[2048,256]{1,0:T(8,128)(2,1)}, u32[]{:S(2)}) copy-start(bf16[2048,256]{1,0:T(8,128)(2,1)} %param.21) | copy-start | bytes 3145732
  28.5 21.7 %copy-start.9 = (bf16[128]{0:T(256)(128)(2,1)S(1)}, bf16[128]{0:T(256)(128)(2,1)}, u32[]{:S(2)}) copy-start(bf16[128]{0:T(256)(128)(2,1)} %param.23) | copy-start | bytes 772
  28.5 21.7 %copy-start.5 = (s32[16,4]{0,1:T(4,128)S(1)}, s32[16,4]{0,1:T(4,128)}, u32[]{:S(2)}) copy-start(s32[16,4]{0,1:T(4,128)} %param.32) | copy-start | bytes 772
  28.5 22.4 %copy-start.4 = (bf16[2048]{0:T(1024)(128)(2,1)S(1)}, bf16[2048]{0:T(1024)(128)(2,1)}, u32[]{:S(2)}) copy-start(bf16[2048]{0:T(1024)(128)(2,1)} %param.28) | copy-start | bytes 12292
  28.6 22.5 %copy-start.7 = (s32[16]{0:T(128)S(1)}, s32[16]{0:T(128)}, u32[]{:S(2)}) copy-start(s32[16]{0:T(128)} %param.27) | copy-start | bytes 196
  301.0 11.3 %copy-start.6 = (f32[16,4]{0,1:T(4,128)S(1)}, f32[16,4]{0,1:T(4,128)}, u32[]{:S(2)}) copy-start(f32[16,4]{0,1:T(4,128)} %param.33) | copy-start | bytes 772
  306.7 35.6 %all-to-all-start.3 = ((bf16[16,2,1,4,2048]{4,3,1,2,0:T(4,128)(2,1)}), bf16[16,2,1,4,2048]{4,3,1,2,0:T(4,128)(2,1)S(1)}, u32[]{:S(2)}, u32[]{:S(2)}) async-start(bf16[16,2,1,4,2048]{4,3,1,2,0:T(4,128)(2,1)} %copy.94), calls=%async_computation.3 | async-start | bytes 1048576 | tf_op jit(solution)/shard_map/all_to_all | solution.py:35
Sparse Core Ops, SparseCore 0:
  29.7 142.2 all-gather.1
